TPU v7x, 768 devices: a whole 4x8x12 slice. The times are simulated.
768 devices in a mesh: ep: 24 (over z, core), tp: 32 (over y, x).
Axes of the slice: x: 4, y: 8, z: 12, core: 2. Of those that a mesh axis runs over, the one named last changes fastest.
Arguments:
- tokens: bfloat16 [3072, 2048], P('ep', 'tp'), may hold values from -6 to 6
- out_grad: bfloat16 [3072, 2048], P('ep', 'tp'), may hold values from -6 to 6
- routes: int32 [3072, 2], P('ep'), may hold values from 0 to 23, all different within a row; in each aligned block of 128 rows (0 to 127, 128 to 255, ...) at most 16 rows name the same one
- gates: float32 [3072, 2], P('ep'), may hold values from 0.1 to 0.9
- gate_weight: bfloat16 [24, 2048, 5632], P('ep', None, 'tp'), may hold values from -0.125 to 0.125
- up_weight: bfloat16 [24, 2048, 5632], P('ep', None, 'tp'), may hold values from -0.125 to 0.125
- down_weight: bfloat16 [24, 5632, 2048], P('ep', 'tp'), may hold values from -0.078125 to 0.078125
Outputs:
- tokens_grad: bfloat16 [3072, 2048], P('ep', 'tp')
- gates_grad: float32 [3072, 2], P(('ep', 'tp'))
- gate_weight_grad: bfloat16 [24, 2048, 5632], P('ep', None, 'tp')
- up_weight_grad: bfloat16 [24, 2048, 5632], P('ep', None, 'tp')
- down_weight_grad: bfloat16 [24, 5632, 2048], P('ep', 'tp')
Inputs may be any that keep to these rules, and one draw needn't show every extreme that they name: `routes`: the 2 experts of a token differ. In each aligned block of 128 rows (the tokens of one index of ep) no expert is named by more than 16 rows, a bound that some block reaches.
All inputs are finite; a program needn't handle non-finite values.
Results may differ from a plain program's by a relative error of at most 0.029.
Values may be sent and summed in bfloat16 or wider, within the bound.
No kernel may reach another device: no remote copies, remote signals or barrier semaphores. Data moves between devices by JAX's collectives and lax.ppermute only.
A program may use at most 64 MiB of HBM per device.

v0:
```python
import jax
import jax.numpy as jnp
from jax import lax
from jax.sharding import Mesh
from jax.sharding import PartitionSpec as P

TP = ("tp_0", "tp_1")
EP_TP = ("ep", "tp_0", "tp_1")


def in_one_piece(arrays, axis, split_dim, concat_dim, along):
    both = jnp.concatenate(arrays, axis=along)
    filled, at, done = (
        lax.all_to_all(both, axis, split_axis=split_dim, concat_axis=concat_dim, tiled=True),
        0,
        [],
    )
    for a in arrays:
        done.append(lax.slice_in_dim(filled, at, at + a.shape[along], axis=along))
        at += a.shape[along]
    return tuple(done)


def rows_first(arrays, axis, dims):
    turned = [jnp.moveaxis(a, dim, 0) for a, dim in zip(arrays, dims)]
    widths = [t[0].size for t in turned]
    both = jnp.concatenate([t.reshape(-1, w) for t, w in zip(turned, widths)], axis=1)
    filled = lax.all_gather(both, axis, axis=0, tiled=True)
    pieces = jnp.split(filled, [sum(widths[:k]) for k in range(1, len(widths))], axis=1)
    return tuple(
        (
            jnp.moveaxis(b.reshape(-1, *t.shape[1:]), 0, dim)
            for b, t, dim in zip(pieces, turned, dims)
        )
    )


def copy_for_each(array, axis):
    length = lax.axis_size(axis)
    return lax.all_to_all(
        jnp.broadcast_to(array[None], (length, *array.shape)), axis, 0, 0, tiled=True
    )


def of_everyone(array, axis):
    everything = copy_for_each(array, axis)
    return jnp.sum(everything, axis=0)


def scatter_axes(array, axes, dim):
    if not axes:
        return array
    nearer = lax.psum_scatter(array, axes[0], scatter_dimension=dim, tiled=True)
    return scatter_axes(nearer, axes[1:], dim)


def expert_grads(rows, cotan, w_gate, w_up, w_down):
    pre_gate = jnp.dot(rows, w_gate, preferred_element_type=jnp.float32)
    pre_up = jnp.dot(rows, w_up, preferred_element_type=jnp.float32)
    activated = jax.nn.silu(pre_gate)
    hidden = (activated * pre_up).astype(jnp.bfloat16)
    hid_grad = jnp.dot(cotan, w_down.T, preferred_element_type=jnp.float32)
    sigmoid_gate = jax.nn.sigmoid(pre_gate)
    gate_part = (hid_grad * pre_up * sigmoid_gate * (1.0 + pre_gate * (1.0 - sigmoid_gate))).astype(
        jnp.bfloat16
    )
    up_part = (hid_grad * activated).astype(jnp.bfloat16)
    slot_dots = jnp.sum(hidden.astype(jnp.float32) * hid_grad, axis=1)
    down_grad = jnp.dot(hidden.T, cotan, preferred_element_type=jnp.float32).astype(jnp.bfloat16)
    gate_grad = jnp.dot(rows.T, gate_part, preferred_element_type=jnp.float32).astype(jnp.bfloat16)
    up_grad = jnp.dot(rows.T, up_part, preferred_element_type=jnp.float32).astype(jnp.bfloat16)
    return (gate_part, up_part, slot_dots, gate_grad, up_grad, down_grad)


def on_device(tokens, out_grad, routes, gates, gate_weight, up_weight, down_weight):
    tok_dev, top_k = routes.shape
    ep_size = lax.axis_size("ep")
    tp_size = lax.axis_size(TP)
    capacity = (3 * tok_dev + ep_size - 1) // ep_size
    buffer_rows = ep_size * capacity
    slice_width = tokens.shape[1]
    flat_expert = routes.reshape(-1)
    onehot = (flat_expert[:, None] == jnp.arange(ep_size, dtype=jnp.int32)[None, :]).astype(
        jnp.int32
    )
    slot_rank = jnp.sum((jnp.cumsum(onehot, axis=0) - onehot) * onehot, axis=1)
    slot_dest = flat_expert * capacity + slot_rank
    placed = jnp.arange(buffer_rows, dtype=jnp.int32)[:, None] == slot_dest[None, :]
    placed_float = placed.astype(jnp.float32)
    select = jnp.any(placed.reshape(buffer_rows, tok_dev, top_k), axis=2).astype(jnp.bfloat16)
    slot_gate = jnp.dot(placed_float, gates.reshape(-1), precision=lax.Precision.HIGHEST)
    sent_rows = jnp.dot(select, tokens, preferred_element_type=jnp.float32).astype(jnp.bfloat16)
    cotan_rows = jnp.dot(select, out_grad, preferred_element_type=jnp.float32)
    sent_cotan = (slot_gate[:, None] * cotan_rows).astype(jnp.bfloat16)
    recv_rows, recv_cotan = in_one_piece(
        (
            sent_rows.reshape(ep_size, capacity, slice_width),
            sent_cotan.reshape(ep_size, capacity, slice_width),
        ),
        "ep",
        0,
        0,
        1,
    )
    whole_rows, whole_cotan = rows_first((recv_rows, recv_cotan), TP, (2, 2))
    model_width = whole_rows.shape[2]
    rows = whole_rows.reshape(buffer_rows, model_width)
    cotan = whole_cotan.reshape(buffer_rows, model_width)
    w_gate = gate_weight[0]
    w_up = up_weight[0]
    gate_part, up_part, slot_dots, gate_grad, up_grad, down_grad = expert_grads(
        rows, cotan, w_gate, w_up, down_weight[0]
    )
    partial_value = jnp.dot(gate_part, w_gate.T, preferred_element_type=jnp.float32)
    partial_value = (
        partial_value + jnp.dot(up_part, w_up.T, preferred_element_type=jnp.float32)
    ).astype(jnp.bfloat16)
    share = tok_dev // tp_size
    start = lax.axis_index(TP) * share
    summed = of_everyone(slot_dots, TP)
    row_sums = scatter_axes(partial_value.reshape(ep_size, capacity, model_width), TP, 2).astype(
        jnp.float32
    )
    back_rows, back_dots = (
        lax.all_to_all(
            row_sums.astype(jnp.bfloat16), "ep", split_axis=0, concat_axis=0, tiled=True
        ).astype(row_sums.dtype),
        lax.all_to_all(
            summed.reshape(ep_size, capacity).astype(jnp.bfloat16),
            "ep",
            split_axis=0,
            concat_axis=0,
            tiled=True,
        ).astype(jnp.float32),
    )
    slot_rows = back_rows.reshape(buffer_rows, slice_width)[slot_dest]
    tokens_grad = jnp.sum(slot_rows.reshape(tok_dev, top_k, slice_width), axis=1).astype(
        jnp.bfloat16
    )
    token_dots = back_dots.reshape(buffer_rows)[slot_dest].reshape(tok_dev, top_k)
    own_dots = lax.dynamic_slice_in_dim(token_dots, start, share, 0)
    own_gates = lax.dynamic_slice_in_dim(gates, start, share, 0)
    gates_grad = own_dots / own_gates
    return (tokens_grad, gates_grad, gate_grad[None], up_grad[None], down_grad[None])


def solution(mesh):
    torus = Mesh(mesh.devices.reshape(mesh.shape["ep"], 8, 4), ("ep", "tp_0", "tp_1"))
    return jax.shard_map(
        on_device,
        mesh=torus,
        in_specs=(
            P("ep", TP),
            P("ep", TP),
            P("ep", None),
            P("ep", None),
            P("ep", None, TP),
            P("ep", None, TP),
            P("ep", TP, None),
        ),
        out_specs=(
            P("ep", TP),
            P(EP_TP, None),
            P("ep", None, TP),
            P("ep", None, TP),
            P("ep", TP, None),
        ),
        check_vma=False,
    )
```

profile of v0, /device:TPU:1, one launch (start us, length us, event | category | flops | bytes accessed | tf_op | source)
XLA Modules:
  0.0 251.6 jit_solution(3340359028984912341)
XLA Ops:
  7.2 0.0 all-gather.2.cloned.1.call-start
  7.2 0.8 copy.51
  8.1 0.1 eq.46
  8.2 0.1 eq.50
  8.4 0.6 reduce-window.6
  9.0 0.2 slice_reduce_fusion
  9.2 0.1 fusion.24
  9.3 0.1 reduce_sum.41
  9.4 0.8 copy.57
  10.2 0.1 reshape.175
  10.4 0.1 copy.55
  10.5 0.1 fusion.19
  10.5 0.9 convolution_convert_fusion.3
  11.4 0.1 copy.56
  11.5 0.3 convolution_reduce_fusion
  11.9 0.9 fusion.12
  12.7 0.1 copy.58
  12.9 0.2 reshape.189
  13.1 27.5 %all_to_all.22 = bf16[24,2,1024]{2,1,0:T(2,128)(2,1)S(1)} all-to-all(bf16[24,2,1024]{2,1,0:T(2,128)(2,1)S(1)} %reshape.189), channel_id=1, replica_groups=mesh['ep'=24,'tp_0'=8,'tp_1'=4] {'ep'}, dimensions={0} | all-to-all | bytes 196608 | tf_op jit(solution)/shard_map/all_to_all | solution.py:14
  40.6 0.2 reshape.190
  40.8 0.8 copy.59
  41.6 0.0 all-gather.2.cloned.1.call-update
  41.6 0.0 reduce-scatter.5.cloned.1.call-start
  41.7 81.2 %all-gather.2.cloned.1.call-done = bf16[2048,768]{1,0:T(8,128)(2,1)} async-done(((bf16[64,768]{1,0:T(8,128)(2,1)}), bf16[2048,768]{1,0:T(8,128)(2,1)}) %all-gather.2.cloned.1.call-update) | async-done | bytes 3145744 | tf_op jit(solution)/shard_map/all_gather | solution.py:28
  122.9 3.3 %fusion.27 = (bf16[2048,384]{1,0:T(8,128)(2,1)S(1)}, bf16[2048,384]{1,0:T(8,128)(2,1)}) fusion(bf16[2048,768]{1,0:T(8,128)(2,1)} %all-gather.2.cloned.1.call-done), kind=kLoop, calls=%fused_computation.57 | loop fusion | bytes 6291456 | tf_op jit(solution)/shard_map/split | solution.py:29
  126.2 1.6 copy.71
  127.8 1.7 copy.70
  129.6 0.7 fusion.8
  130.2 0.4 copy-done.2
  130.7 0.7 fusion.10
  131.3 0.7 copy-done.1
  132.1 0.2 copy-done.3
  132.2 0.7 multiply_reduce_fusion
  133.0 0.6 fusion.13
  133.6 1.8 add_convert_fusion
  135.3 0.0 reduce-scatter.5.cloned.1.call-update
  135.3 0.0 reduce-scatter.7.cloned.1.call-start
  135.4 0.1 mul.80
  135.6 42.7 %reduce-scatter.5.cloned.1.call-done = bf16[24,16,256]{2,1,0:T(8,128)(2,1)} async-done(((bf16[24,16,2048]{2,1,0:T(8,128)(2,1)}), bf16[24,16,256]{2,1,0:T(8,128)(2,1)}) %reduce-scatter.5.cloned.1.call-update) | async-done | bytes 196624 | tf_op jit(solution)/shard_map/reduce_scatter | solution.py:53
  178.2 2.5 copy.67
  180.7 3.0 %reshape.178 = bf16[256,384]{1,0:T(8,128)(2,1)} reshape(bf16[256,24,16]{2,1,0:T(8,128)(2,1)} %bitcast.91) | data formatting | bytes 393216
  183.8 1.4 fusion.1
  185.2 0.6 broadcast_in_dim.8
  185.8 7.6 %all-to-all-start.2 = ((f32[32,1,384]{2,1,0:T(1,128)}), f32[32,1,384]{2,1,0:T(1,128)S(1)}, u32[]{:S(2)}, u32[]{:S(2)}) async-start(f32[32,1,384]{2,1,0:T(1,128)} %broadcast_in_dim.8), calls=%async_computation.3 | async-start | bytes 98304 | tf_op jit(solution)/shard_map/all_to_all | solution.py:40
  193.4 1.4 fusion.2
  194.8 7.3 %all-to-all-done.2 = f32[32,1,384]{2,1,0:T(1,128)S(1)} async-done(((f32[32,1,384]{2,1,0:T(1,128)}), f32[32,1,384]{2,1,0:T(1,128)S(1)}, u32[]{:S(2)}, u32[]{:S(2)}) %all-to-all-start.2) | async-done | bytes 49184 | tf_op jit(solution)/shard_map/all_to_all | solution.py:40
  202.1 0.1 reduce_sum.45
  202.2 0.7 convert_element_type.83
  202.9 15.7 %all-to-all-start.3 = ((bf16[24,1,16]{2,1,0:T(2,128)(2,1)}), bf16[24,1,16]{2,1,0:T(2,128)(2,1)S(1)}, u32[]{:S(2)}, u32[]{:S(2)}) async-start(bf16[24,1,16]{2,1,0:T(2,128)(2,1)} %convert_element_type.83), calls=%async_computation.4 | async-start | bytes 24576 | tf_op jit(solution)/shard_map/all_to_all | solution.py:128
  218.6 2.8 %fusion = bf16[1,176,2048]{2,1,0:T(8,128)(2,1)} fusion(bf16[384,176]{0,1:T(8,128)(2,1)S(1)} %get-tuple-element.26, bf16[2048,384]{0,1:T(8,128)(2,1)} %copy.71), kind=kOutput, calls=%fused_computation.6 | convolution fusion | flops 277184512 | bytes 2428928 | tf_op jit(solution)/shard_map/dot_general | solution.py:69
  221.5 1.1 reshape.179
  222.6 0.3 copy.68
  222.8 0.7 reshape.191
  223.6 4.4 %all-to-all-done.3 = bf16[24,1,16]{2,1,0:T(2,128)(2,1)S(1)} async-done(((bf16[24,1,16]{2,1,0:T(2,128)(2,1)}), bf16[24,1,16]{2,1,0:T(2,128)(2,1)S(1)}, u32[]{:S(2)}, u32[]{:S(2)}) %all-to-all-start.3) | async-done | bytes 800 | tf_op jit(solution)/shard_map/all_to_all | solution.py:128
  228.0 5.3 %all-to-all-start.1 = ((bf16[24,2,512]{2,1,0:T(2,128)(2,1)}), bf16[24,2,512]{2,1,0:T(2,128)(2,1)S(1)}, u32[]{:S(2)}, u32[]{:S(2)}) async-start(bf16[24,2,512]{2,1,0:T(2,128)(2,1)} %reshape.191), calls=%async_computation.2 | async-start | bytes 98304 | tf_op jit(solution)/shard_map/all_to_all | solution.py:125
  233.3 0.1 reshape.158
  233.4 1.9 gather_fusion.1
  235.4 0.1 reshape.155
  235.5 0.6 copy.66
  236.2 7.2 %all-to-all-done.1 = bf16[24,2,512]{2,1,0:T(2,128)(2,1)S(1)} async-done(((bf16[24,2,512]{2,1,0:T(2,128)(2,1)}), bf16[24,2,512]{2,1,0:T(2,128)(2,1)S(1)}, u32[]{:S(2)}, u32[]{:S(2)}) %all-to-all-start.1) | async-done | bytes 49184 | tf_op jit(solution)/shard_map/all_to_all | solution.py:125
  243.3 0.1 reshape.192
  243.5 0.7 gather_fusion
  244.2 0.2 reduce_sum.43
  244.4 0.7 copy.65
  (20 shorter events, 0.3 us)
Async XLA Ops:
  7.2 122.4 %copy-start = (bf16[1,2048,176]{1,2,0:T(8,128)(2,1)S(1)}, bf16[1,2048,176]{1,2,0:T(8,128)(2,1)}, u32[]{:S(2)}) copy-start(bf16[1,2048,176]{1,2,0:T(8,128)(2,1)} %param.11) | copy-start | bytes 2162692
  7.2 115.7 %all-gather.2.cloned.1.call-start = ((), (), s32[]{:S(2)}) async-start(), calls=%async_computation.6 | async-start | bytes 3244032 | tf_op jit(solution)/shard_map/all_gather | solution.py:28
  41.6 136.6 %reduce-scatter.5.cloned.1.call-start = ((), (), s32[]{:S(2)}) async-start(), calls=%async_computation.7 | async-start | bytes 1769472 | tf_op jit(solution)/shard_map/reduce_scatter | solution.py:53
  129.5 1.1 copy-start.2
  130.7 1.4 copy-start.1
  130.7 1.6 copy-start.3
  135.3 86.1 %reduce-scatter.7.cloned.1.call-start = ((), (), s32[]{:S(2)}) async-start(), calls=%async_computation.8 | async-start | bytes 245760
  185.8 16.3 %all-to-all-start.2 = ((f32[32,1,384]{2,1,0:T(1,128)}), f32[32,1,384]{2,1,0:T(1,128)S(1)}, u32[]{:S(2)}, u32[]{:S(2)}) async-start(f32[32,1,384]{2,1,0:T(1,128)} %broadcast_in_dim.8), calls=%async_computation.3 | async-start | bytes 98304 | tf_op jit(solution)/shard_map/all_to_all | solution.py:40
  202.9 25.1 %all-to-all-start.3 = ((bf16[24,1,16]{2,1,0:T(2,128)(2,1)}), bf16[24,1,16]{2,1,0:T(2,128)(2,1)S(1)}, u32[]{:S(2)}, u32[]{:S(2)}) async-start(bf16[24,1,16]{2,1,0:T(2,128)(2,1)} %convert_element_type.83), calls=%async_computation.4 | async-start | bytes 24576 | tf_op jit(solution)/shard_map/all_to_all | solution.py:128
  228.0 15.3 %all-to-all-start.1 = ((bf16[24,2,512]{2,1,0:T(2,128)(2,1)}), bf16[24,2,512]{2,1,0:T(2,128)(2,1)S(1)}, u32[]{:S(2)}, u32[]{:S(2)}) async-start(bf16[24,2,512]{2,1,0:T(2,128)(2,1)} %reshape.191), calls=%async_computation.2 | async-start | bytes 98304 | tf_op jit(solution)/shard_map/all_to_all | solution.py:125
Sparse Core Ops, SparseCore 0:
  41.8 81.0 all-gather.1
  135.5 42.7 reduce-scatter.4
  183.9 29.8 reduce-scatter.6
where the time goes:
time: 252 us
  waiting for transfers between devices  143 us (57%)
  starting transfers between devices  28.7 us (11%)
  blocking collectives  27.5 us (11%)
  local copies, waits for them, and re-layouts  25.3 us (10%)
  between operations  14 us (6%)
  matrix products  12.1 us (5%)
    all_gather x1, waiting for transfers between devices, rows_first(): filled = lax.all_gather(both, axis, axis=0, tiled=True)  81.2 us
    reduce_scatter x1, waiting for transfers between devices, scatter_axes(): nearer = lax.psum_scatter(array, axes[0], scatter_dimension=dim, tiled=True)  42.7 us
    all_to_all x1, blocking collectives, in_one_piece(): lax.all_to_all(both, axis, split_axis=split_dim, concat_axis=concat_dim,...  27.5 us
    unnamed x22, local copies, waits for them, and re-layouts  15.8 us
    all_to_all x1, starting transfers between devices, on_device(): lax.all_to_all(summed.reshape(ep_size, capacity).astype(jnp.bfloat16), 'e...  15.7 us
    all_to_all x1, starting transfers between devices, copy_for_each(): lax.all_to_all(jnp.broadcast_to(array[None], (length, *array.shape)), axi...  7.58 us
    all_to_all x1, waiting for transfers between devices, copy_for_each(): lax.all_to_all(jnp.broadcast_to(array[None], (length, *array.shape)), axi...  7.33 us
    all_to_all x1, waiting for transfers between devices, on_device(): lax.all_to_all(row_sums.astype(jnp.bfloat16), 'ep', split_axis=0, concat_...  7.16 us
  transfers between devices with their start and end apart: 6, of which 5 were waited for; matrix products, arithmetic and copies ran while one was open for 5% of the time, Pallas kernels for 0%

commit v1 on v0

v1 whole, which is shorter than its diff:
```python
import jax
import jax.numpy as jnp
from jax import lax
from jax.sharding import Mesh
from jax.sharding import PartitionSpec as P

TP = ("y", "x")
BF16 = jnp.bfloat16
F32 = jnp.float32


def exchange(array, axis):
    return lax.all_to_all(array, axis, split_axis=0, concat_axis=0, tiled=True)


def to_all(array, axis):
    copies = jnp.broadcast_to(array[None], (lax.axis_size(axis), *array.shape))
    return exchange(copies, axis)


def two_rows(values):
    high = values.astype(BF16)
    low = (values - high.astype(F32)).astype(BF16)
    return jnp.concatenate([high[..., None, :], low[..., None, :]], axis=-2)


def add_up(parts):
    total = jnp.sum(parts.astype(F32), axis=0)
    dots = total[..., -8, :] + total[..., -7, :]
    return total[..., :-8, :], dots


def with_dots(rows, dots):
    pad = [(0, 0)] * (rows.ndim - 2) + [(0, 6), (0, 0)]
    return jnp.concatenate([rows.astype(BF16), jnp.pad(two_rows(dots), pad)], axis=-2)


def on_device(tokens, out_grad, routes, gates, gate_weight, up_weight, down_weight):
    tok_dev, top_k = routes.shape
    n_ep, n_y, n_x = lax.axis_size("ep"), lax.axis_size("y"), lax.axis_size("x")
    cap = (3 * tok_dev + n_ep - 1) // n_ep
    rows = n_ep * cap
    feats = tokens.shape[1]
    width = n_y * n_x * feats
    flat = routes.T.reshape(-1)
    slots = flat.shape[0]
    before = jnp.arange(slots)[None, :] < jnp.arange(slots)[:, None]
    same = (flat[None, :] == flat[:, None]) & before
    dest = (flat * cap + jnp.sum(same.astype(jnp.int32), axis=1)).reshape(top_k, tok_dev)
    place = jnp.arange(rows, dtype=jnp.int32)[:, None]
    at = [place == dest[k][None, :] for k in range(top_k)]
    select = (at[0] | at[1]).astype(BF16)
    slot_gate = sum(jnp.sum(jnp.where(at[k], gates[:, k][None, :], 0.0), axis=1) for k in range(top_k))
    both = jnp.dot(select, jnp.concatenate([tokens, out_grad], axis=1), preferred_element_type=F32)
    scale = jnp.where(jnp.arange(2 * feats)[None, :] < feats, 1.0, slot_gate[:, None])
    sent = (both * scale).astype(BF16)

    got = exchange(sent.reshape(n_ep, cap, 2 * feats), "ep").reshape(rows, 2 * feats)
    by_y = to_all(got.T, "y")
    by_xy = to_all(by_y, "x").reshape(n_x, n_y, 2, feats, rows)
    x_t = by_xy[:, :, 0].transpose(1, 0, 2, 3).reshape(width, rows)
    c_t = by_xy[:, :, 1].transpose(1, 0, 2, 3).reshape(width, rows)

    w_gate, w_up, w_down = gate_weight[0].T, up_weight[0].T, down_weight[0]
    pre_gate = jnp.dot(w_gate, x_t, preferred_element_type=F32)
    pre_up = jnp.dot(w_up, x_t, preferred_element_type=F32)
    hid_grad = jnp.dot(w_down, c_t, preferred_element_type=F32)
    sig = jax.nn.sigmoid(pre_gate)
    act = pre_gate * sig
    hidden = (act * pre_up).astype(BF16)
    gate_part = (hid_grad * pre_up * sig * (1.0 + pre_gate * (1.0 - sig))).astype(BF16)
    up_part = (hid_grad * act).astype(BF16)
    dots = jnp.sum(hidden.astype(F32) * hid_grad, axis=0)

    def dot_t(a, b, dims):
        return lax.dot_general(a, b, (dims, ((), ())), preferred_element_type=F32)

    piece = dot_t(w_gate, gate_part, ((0,), (0,))) + dot_t(w_up, up_part, ((0,), (0,)))
    piece = piece.astype(BF16).reshape(n_y, n_x, feats, rows).transpose(1, 0, 2, 3)
    chunks = with_dots(piece, jnp.broadcast_to(dots, (n_x, n_y, rows)))
    near, near_dots = add_up(exchange(chunks, "x"))

    gate_grad = dot_t(gate_part, x_t, ((1,), (1,))).astype(BF16)
    up_grad = dot_t(up_part, x_t, ((1,), (1,))).astype(BF16)
    down_grad = dot_t(hidden, c_t, ((1,), (1,))).astype(BF16)

    row_sum, all_dots = add_up(exchange(with_dots(near, near_dots), "y"))
    packed = jnp.concatenate([row_sum.astype(BF16), two_rows(all_dots)], axis=0)
    packed = jnp.pad(packed, ((0, 2 * feats - packed.shape[0]), (0, 0))).T
    back = exchange(packed.reshape(n_ep, cap, 2 * feats), "ep").reshape(rows, 2 * feats)
    tokens_grad = dot_t(select, back, ((0,), (0,)))[:, :feats].astype(BF16)
    share = tok_dev // (n_y * n_x)
    start = lax.axis_index(TP) * share
    own_dest = lax.dynamic_slice_in_dim(dest, start, share, 1).T
    own_gates = lax.dynamic_slice_in_dim(gates, start, share, 0)
    back_dots = back[:, feats].astype(F32) + back[:, feats + 1].astype(F32)
    mine = own_dest[:, :, None] == jnp.arange(rows, dtype=jnp.int32)
    own_dots = jnp.sum(jnp.where(mine, back_dots, 0.0), axis=2)
    return (
        tokens_grad,
        own_dots / own_gates,
        gate_grad.T[None],
        up_grad.T[None],
        down_grad[None],
    )


def solution(mesh):
    torus = Mesh(mesh.devices.reshape(mesh.shape["ep"], 8, 4), ("ep", "y", "x"))
    return jax.shard_map(
        on_device,
        mesh=torus,
        in_specs=(
            P("ep", TP),
            P("ep", TP),
            P("ep", None),
            P("ep", None),
            P("ep", None, TP),
            P("ep", None, TP),
            P("ep", TP, None),
        ),
        out_specs=(
            P("ep", TP),
            P(("ep", "y", "x"), None),
            P("ep", None, TP),
            P("ep", None, TP),
            P("ep", TP, None),
        ),
        check_vma=False,
    )
```

time: 252 us -> 176 us (0.70)
  waiting for transfers between devices: 143 us -> 15.8 us
  blocking collectives: 27.5 us -> 117 us
  local copies, waits for them, and re-layouts: 25.3 us -> 8.37 us
  between operations: 14 us -> 0.9 us
  starting transfers between devices: 28.7 us -> 16.6 us
  other arithmetic: 1.22 us -> 5.76 us
    all_to_all x1 -> x4, blocking collectives: 27.5 us -> 117 us  [exchange(): return lax.all_to_all(array, axis, split_axis=0, concat_axis=0, tiled=True)]
    all_gather x1 -> x0, waiting for transfers between devices: 81.2 us -> none  [rows_first(): filled = lax.all_gather(both, axis, axis=0, tiled=True)]
    reduce_scatter x1 -> x0, waiting for transfers between devices: 42.7 us -> none  [scatter_axes(): nearer = lax.psum_scatter(array, axes[0], scatter_dimension=dim, tiled=True)]
    unnamed x22 -> x13, local copies, waits for them, and re-layouts: 15.8 us -> 1.87 us
    all_to_all x3 -> x2, starting transfers between devices: 28.6 us -> 16.6 us  [exchange(): return lax.all_to_all(array, axis, split_axis=0, concat_axis=0, tiled=True)]
    split x1 -> x0, local copies, waits for them, and re-layouts: 3.33 us -> none  [rows_first(): jnp.split(filled, [sum(widths[:k]) for k in range(1, len(widths))], axis=1)]
    all_to_all x3 -> x2, waiting for transfers between devices: 18.9 us -> 15.8 us  [exchange(): return lax.all_to_all(array, axis, split_axis=0, concat_axis=0, tiled=True)]
    gather x2 -> x0, local copies, waits for them, and re-layouts: 2.68 us -> none  [the longest x1 1.95 us: on_device(): back_dots.reshape(buffer_rows)[slot_dest].reshape(tok_dev, top_k)]
  transfers between devices with their start and end apart: 6 -> 2, of which waited for: 5 -> 2; matrix products, arithmetic and copies ran while one was open for 5% -> 3% of each run, Pallas kernels for 0% -> 0%
where the time goes in v1:
time: 176 us; the launch traced here: 175 us
  blocking collectives  117 us (66%)
  starting transfers between devices  16.6 us (9%)
  waiting for transfers between devices  15.8 us (9%)
  matrix products  11.3 us (6%)
  local copies, waits for them, and re-layouts  8.37 us (5%)
  other arithmetic  5.76 us (3%)
    all_to_all x4, blocking collectives, exchange(): return lax.all_to_all(array, axis, split_axis=0, concat_axis=0, tiled=True)  117 us
    all_to_all x2, starting transfers between devices, exchange(): return lax.all_to_all(array, axis, split_axis=0, concat_axis=0, tiled=True)  16.6 us
    all_to_all x2, waiting for transfers between devices, exchange(): return lax.all_to_all(array, axis, split_axis=0, concat_axis=0, tiled=True)  15.8 us
    dot_general x6, matrix products, dot_t(): return lax.dot_general(a, b, (dims, ((), ())), preferred_element_type=F32)  8.65 us
  transfers between devices with their start and end apart: 2, of which 2 were waited for; matrix products, arithmetic and copies ran while one was open for 3% of the time, Pallas kernels for 0%

profile of v1, /device:TPU:1, one launch (start us, length us, event | category | flops | bytes accessed | tf_op | source)
XLA Modules:
  0.0 175.4 jit_solution(16154286335720403128)
XLA Ops:
  0.6 0.0 copy-start
  0.7 0.9 convert_reduce_fusion.2
  1.6 0.7 multiply_add_fusion
  2.3 0.8 slice_bitcast_fusion.2
  3.1 0.2 select_reduce_fusion
  3.3 0.9 fusion.4
  4.2 27.5 %all_to_all.30 = bf16[24,16,128]{2,1,0:T(8,128)(2,1)S(1)} all-to-all(bf16[24,16,128]{2,1,0:T(8,128)(2,1)S(1)} %bitcast.89), channel_id=1, replica_groups=mesh['ep'=24,'y'=8,'x'=4] {'ep'}, dimensions={0} | all-to-all | bytes 196608 | tf_op jit(solution)/shard_map/all_to_all | solution.py:13
  31.7 0.1 copy.41
  31.8 0.1 broadcast_in_dim.97
  31.9 28.4 %all_to_all.31 = bf16[8,128,384]{2,1,0:T(8,128)(2,1)S(1)} all-to-all(bf16[8,128,384]{2,1,0:T(8,128)(2,1)S(1)} %broadcast_in_dim.97), channel_id=1, replica_groups=mesh['ep'=24,'y'=8,'x'=4] {'y'}, dimensions={0} | all-to-all | bytes 1572864 | tf_op jit(solution)/shard_map/all_to_all | solution.py:13
  60.3 0.5 broadcast_in_dim.98
  60.8 38.9 %all_to_all.32 = bf16[4,8,128,384]{3,2,1,0:T(8,128)(2,1)S(1)} all-to-all(bf16[4,8,128,384]{3,2,1,0:T(8,128)(2,1)S(1)} %broadcast_in_dim.98), channel_id=1, replica_groups=mesh['ep'=24,'y'=8,'x'=4] {'x'}, dimensions={0} | all-to-all | bytes 6291456 | tf_op jit(solution)/shard_map/all_to_all | solution.py:13
  99.7 0.4 slice_bitcast_fusion
  100.1 0.0 copy-start.2
  100.1 0.2 copy.43
  100.3 0.9 copy-done.2
  101.2 0.6 convolution_bitcast_fusion.1
  101.8 0.0 copy-done
  101.8 0.5 convolution_bitcast_fusion
  102.4 0.0 copy-start.5
  102.4 0.2 copy.42
  102.6 0.0 copy-start.1
  102.6 0.9 copy-done.5
  103.5 0.6 multiply_reduce_fusion
  104.1 0.0 copy-done.1
  104.1 0.6 fusion.6
  104.7 1.8 %fusion = bf16[2048,384]{0,1:T(8,128)(2,1)} fusion(f32[384,2048]{1,0:T(8,128)S(1)} %fusion.6, bf16[176,384]{1,0:T(8,128)(2,1)S(1)} %get-tuple-element.14, bf16[1,2048,176]{1,2,0:T(8,128)(2,1)S(1)} %copy-done.2), kind=kOutput, calls=%fused_computation.2 | convolution fusion | flops 278396928 | bytes 5574656 | tf_op jit(solution)/shard_map/dot_general | solution.py:76
  106.5 2.6 %copy.44 = bf16[2048,384]{1,0:T(8,128)(2,1)} copy(bf16[2048,384]{0,1:T(8,128)(2,1)} %fusion) | data formatting | bytes 3145728 | tf_op jit(solution)/shard_map/convert_element_type | solution.py:79
  109.1 0.1 fusion.17
  109.3 1.6 pad_maximum_fusion
  110.9 0.2 copy.45
  111.1 21.9 %all_to_all.33 = bf16[4,8,72,384]{3,2,1,0:T(8,128)(2,1)S(1)} all-to-all(bf16[4,8,72,384]{3,2,1,0:T(8,128)(2,1)S(1)} %copy.45), channel_id=1, replica_groups=mesh['ep'=24,'y'=8,'x'=4] {'x'}, dimensions={0} | all-to-all | bytes 3538944 | tf_op jit(solution)/shard_map/all_to_all | solution.py:13
  133.0 0.3 convert_reduce_fusion
  133.3 0.0 copy-start.3
  133.4 0.8 fusion.12
  134.2 4.1 %all-to-all-start.4 = ((bf16[8,72,384]{2,1,0:T(8,128)(2,1)}), bf16[8,72,384]{2,1,0:T(8,128)(2,1)S(1)}, u32[]{:S(2)}, u32[]{:S(2)}) async-start(bf16[8,72,384]{2,1,0:T(8,128)(2,1)} %fusion.12), calls=%async_computation.4 | async-start | bytes 884736 | tf_op jit(solution)/shard_map/all_to_all | solution.py:13
  138.3 0.0 copy-done.3
  138.4 0.1 dynamic-slice_bitcast_fusion
  138.4 1.5 fusion.1
  140.0 9.2 %all-to-all-done.4 = bf16[8,72,384]{2,1,0:T(8,128)(2,1)S(1)} async-done(((bf16[8,72,384]{2,1,0:T(8,128)(2,1)}), bf16[8,72,384]{2,1,0:T(8,128)(2,1)S(1)}, u32[]{:S(2)}, u32[]{:S(2)}) %all-to-all-start.4) | async-done | bytes 442400 | tf_op jit(solution)/shard_map/all_to_all | solution.py:13
  149.2 0.1 convert_reduce_fusion.1
  149.3 0.7 copy.49
  150.1 12.5 %all-to-all-start.5 = ((bf16[24,16,128]{2,1,0:T(8,128)(2,1)}), bf16[24,16,128]{2,1,0:T(8,128)(2,1)S(1)}, u32[]{:S(2)}, u32[]{:S(2)}) async-start(bf16[24,16,128]{2,1,0:T(8,128)(2,1)} %bitcast.25), calls=%async_computation.5 | async-start | bytes 196608 | tf_op jit(solution)/shard_map/all_to_all | solution.py:13
  162.6 3.0 %fusion.3 = bf16[1,176,2048]{2,1,0:T(8,128)(2,1)} fusion(bf16[176,384]{1,0:T(8,128)(2,1)S(1)} %get-tuple-element.8, bf16[2048,384]{1,0:T(8,128)(2,1)} %bitcast.84), kind=kOutput, calls=%fused_computation.8 | convolution fusion | flops 277184512 | bytes 2428928 | tf_op jit(solution)/shard_map/dot_general | solution.py:76
  165.5 0.0 copy-start.4
  165.5 1.5 fusion.2
  167.1 6.5 %all-to-all-done.5 = bf16[24,16,128]{2,1,0:T(8,128)(2,1)S(1)} async-done(((bf16[24,16,128]{2,1,0:T(8,128)(2,1)}), bf16[24,16,128]{2,1,0:T(8,128)(2,1)S(1)}, u32[]{:S(2)}, u32[]{:S(2)}) %all-to-all-start.5) | async-done | bytes 98336 | tf_op jit(solution)/shard_map/all_to_all | solution.py:13
  173.6 0.2 add_reduce_fusion
  173.8 0.2 fusion.22
  174.0 0.6 slice.97
  174.6 0.2 select_reduce_fusion.2
  174.8 0.0 copy-done.4
  174.8 0.6 dynamic-slice_divide_fusion
  (15 shorter events, 0.2 us)
Async XLA Ops:
  0.6 101.2 %copy-start = (bf16[1,2048,176]{1,2,0:T(8,128)(2,1)S(1)}, bf16[1,2048,176]{1,2,0:T(8,128)(2,1)}, u32[]{:S(2)}) copy-start(bf16[1,2048,176]{1,2,0:T(8,128)(2,1)} %param.11) | copy-start | bytes 2162692
  100.1 1.1 copy-start.2
  102.4 1.1 copy-start.5
  102.6 1.5 copy-start.1
  133.3 5.1 %copy-start.3 = (s32[128,2]{0,1:T(2,128)S(1)}, s32[128,2]{0,1:T(2,128)}, u32[]{:S(2)}) copy-start(s32[128,2]{0,1:T(2,128)} %param.9) | copy-start | bytes 3076
  134.2 15.0 %all-to-all-start.4 = ((bf16[8,72,384]{2,1,0:T(8,128)(2,1)}), bf16[8,72,384]{2,1,0:T(8,128)(2,1)S(1)}, u32[]{:S(2)}, u32[]{:S(2)}) async-start(bf16[8,72,384]{2,1,0:T(8,128)(2,1)} %fusion.12), calls=%async_computation.4 | async-start | bytes 884736 | tf_op jit(solution)/shard_map/all_to_all | solution.py:13
  150.1 23.5 %all-to-all-start.5 = ((bf16[24,16,128]{2,1,0:T(8,128)(2,1)}), bf16[24,16,128]{2,1,0:T(8,128)(2,1)S(1)}, u32[]{:S(2)}, u32[]{:S(2)}) async-start(bf16[24,16,128]{2,1,0:T(8,128)(2,1)} %bitcast.25), calls=%async_computation.5 | async-start | bytes 196608 | tf_op jit(solution)/shard_map/all_to_all | solution.py:13
  165.5 9.3 %copy-start.4 = (f32[128,2]{0,1:T(2,128)S(1)}, f32[128,2]{0,1:T(2,128)}, u32[]{:S(2)}) copy-start(f32[128,2]{0,1:T(2,128)} %param.10) | copy-start | bytes 3076
